TPU v7x, 32 devices: a whole 2x2x4 slice. The times are simulated.
32 devices in a mesh: ep: 16 (over z, y, x), tp: 2 (over core).
Axes of the slice: x: 2, y: 2, z: 4, core: 2. Of those that a mesh axis runs over, the one named last changes fastest.
Arguments:
- tokens: bfloat16 [256, 2048], P('ep'), may hold values from -6 to 6
- recurrent_state: float32 [256, 4, 128, 256], P('ep', 'tp'), may hold values from -6 to 6
- query_weight: bfloat16 [2048, 512], P(None, 'tp'), may hold values from -0.125 to 0.125
- key_weight: bfloat16 [2048, 512], P(None, 'tp'), may hold values from -0.125 to 0.125
- decay_weight: bfloat16 [2048, 512], P(None, 'tp'), may hold values from -0.5 to 0.5
- value_weight: bfloat16 [2048, 1024], P(None, 'tp'), may hold values from -0.125 to 0.125
- gate_weight: bfloat16 [2048, 1024], P(None, 'tp'), may hold values from -0.125 to 0.125
- head_gain: float32 [256], replicated, may hold values from 0.1 to 1.9
- output_weight: bfloat16 [1024, 2048], P('tp'), may hold values from -0.375 to 0.375
- norm_gain: float32 [2, 2048], replicated, may hold values from 0.1 to 1.9
- norm_bias: float32 [2, 2048], replicated, may hold values from -1.8 to 1.8
- group_router: bfloat16 [2048, 4], replicated, may hold values from -0.125 to 0.125
- router_weight: bfloat16 [2048, 32], replicated, may hold values from -0.125 to 0.125
- routes: int32 [256, 2], P('ep'), may hold values from 0 to 31, as said below
- expert_gate: bfloat16 [32, 2048, 256], P(('ep', 'tp')), may hold values from -0.125 to 0.125
- expert_up: bfloat16 [32, 2048, 256], P(('ep', 'tp')), may hold values from -0.125 to 0.125
- expert_down: bfloat16 [32, 256, 2048], P(('ep', 'tp')), may hold values from -1.5 to 1.5
Outputs:
- new_tokens: bfloat16 [256, 2048], P('ep', 'tp')
- new_state: float32 [256, 4, 128, 256], P('ep', 'tp')
Inputs may be any that keep to these rules, and one draw needn't show every extreme that they name: `routes`: each row names two different experts of one group (group g holds the experts g * 8 to g * 8 + 7). In the rows of one device each group is named by the same number of rows and no expert by more than 2 rows; some expert is named by exactly 2 rows of every device.
All inputs are finite; a program needn't handle non-finite values.
Results may differ from a plain program's by a relative error of at most 0.01.
Values may be sent and summed in bfloat16 or wider, within the bound.
No kernel may reach another device: no remote copies, remote signals or barrier semaphores. Data moves between devices by JAX's collectives and lax.ppermute only.
A program may use at most 128 MiB of HBM per device.

v0:
```python
import jax
import jax.numpy as jnp
from jax import lax
from jax.sharding import PartitionSpec as P

alpha_res = 2.0**0.5
eps_norm = 1e-05


def layer_normed(inputs, gain_row, bias_row):
    centered = inputs - jnp.mean(inputs, axis=-1, keepdims=True)
    spread = jnp.mean(centered * centered, axis=-1, keepdims=True)
    return centered * lax.rsqrt(spread + eps_norm) * gain_row + bias_row


def on_device(
    tokens,
    recurrent_state,
    query_weight,
    key_weight,
    decay_weight,
    value_weight,
    gate_weight,
    head_gain,
    output_weight,
    norm_gain,
    norm_bias,
    group_router,
    router_weight,
    routes,
    expert_gate,
    expert_up,
    expert_down,
):
    row_count, model_width = tokens.shape
    heads_here = recurrent_state.shape[1]
    key_dim = recurrent_state.shape[2]
    value_dim = recurrent_state.shape[3]

    def project(weight):
        return jnp.dot(tokens, weight, preferred_element_type=jnp.float32)

    queries = project(query_weight).reshape(row_count, heads_here, key_dim) * key_dim ** (-0.5)
    key_rows = project(key_weight).reshape(row_count, heads_here, key_dim)
    value_rows = project(value_weight).reshape(row_count, heads_here, value_dim)
    gate_rows = project(gate_weight)
    decay_rate = jnp.exp(jax.nn.log_sigmoid(project(decay_weight)) / 16.0).reshape(
        row_count, heads_here, key_dim
    )
    new_state = (
        decay_rate[..., None] * recurrent_state + key_rows[..., None] * value_rows[:, :, None, :]
    )
    readout = jnp.sum(queries[..., None] * new_state, axis=2)
    norm_scale = lax.rsqrt(jnp.mean(readout * readout, axis=-1, keepdims=True) + eps_norm)
    gated_rows = (
        (readout * norm_scale * head_gain).reshape(row_count, heads_here * value_dim)
        * jax.nn.silu(gate_rows)
    ).astype(jnp.bfloat16)
    partial_value = jnp.dot(gated_rows, output_weight, preferred_element_type=jnp.float32)
    mixed_sum = lax.psum(partial_value.astype(jnp.bfloat16), "tp").astype(jnp.float32)
    hidden = layer_normed(
        alpha_res * tokens.astype(jnp.float32) + mixed_sum, norm_gain[0], norm_bias[0]
    ).astype(jnp.bfloat16)
    group_count = group_router.shape[1]
    expert_count = router_weight.shape[1]
    per_group = expert_count // group_count
    top_count = routes.shape[1]
    group_logit = jnp.dot(hidden, group_router, preferred_element_type=jnp.float32)
    expert_logit = jnp.dot(hidden, router_weight, preferred_element_type=jnp.float32)
    chosen_group = routes[:, 0] // per_group
    group_hit = chosen_group[:, None] == jnp.arange(group_count, dtype=jnp.int32)[None, :]
    own_logit = jnp.sum(jnp.where(group_hit, group_logit, 0.0), axis=1, keepdims=True)
    group_share = 1.0 / jnp.sum(jnp.exp(group_logit - own_logit), axis=1)
    expert_hit = routes[:, :, None] == jnp.arange(expert_count, dtype=jnp.int32)[None, None, :]
    picked = jnp.sum(jnp.where(expert_hit, expert_logit[:, None, :], 0.0), axis=2)
    route_weight = group_share[:, None] * jax.nn.sigmoid(picked - picked[:, ::-1])
    ep_count = lax.axis_size("ep")
    tp_count = lax.axis_size("tp")
    pair_index = lax.axis_index("tp")
    local_experts = expert_gate.shape[0]
    capacity = 2 * max(1, row_count // expert_count)
    total_slots = expert_count * capacity
    own_slots = total_slots // tp_count
    flat_routes = routes.reshape(row_count * top_count)
    onehot = (flat_routes[:, None] == jnp.arange(expert_count, dtype=jnp.int32)[None, :]).astype(
        jnp.int32
    )
    earlier_count = jnp.sum((jnp.cumsum(onehot, axis=0) - onehot) * onehot, axis=1)
    slot_index = flat_routes * capacity + earlier_count
    pick_all = (slot_index[:, None] == jnp.arange(total_slots, dtype=jnp.int32)[None, :]).astype(
        jnp.bfloat16
    )
    pick_mine = lax.dynamic_slice_in_dim(
        pick_all.reshape(row_count * top_count, ep_count, tp_count, local_experts * capacity),
        pair_index,
        1,
        2,
    ).reshape(row_count * top_count, own_slots)
    outgoing = jnp.einsum(
        "rks,rd->sd",
        pick_mine.reshape(row_count, top_count, own_slots),
        hidden,
        preferred_element_type=jnp.float32,
    ).astype(jnp.bfloat16)
    outgoing = outgoing.reshape(ep_count, local_experts, capacity, model_width)
    col_width = model_width // tp_count
    col_start = pair_index * col_width
    arrived = lax.all_to_all(outgoing, "ep", split_axis=0, concat_axis=0, tiled=True)
    gate_part = jnp.einsum(
        "secd,edf->secf", arrived, expert_gate, preferred_element_type=jnp.float32
    )
    up_part = jnp.einsum("secd,edf->secf", arrived, expert_up, preferred_element_type=jnp.float32)
    activation = (jax.nn.silu(gate_part) * up_part).astype(jnp.bfloat16)
    results = jnp.einsum(
        "secf,efd->secd", activation, expert_down, preferred_element_type=jnp.float32
    ).astype(jnp.bfloat16)
    returned = lax.all_to_all(
        lax.all_to_all(results, "ep", split_axis=0, concat_axis=0, tiled=True),
        "tp",
        split_axis=3,
        concat_axis=1,
        tiled=True,
    )
    fetched = jnp.dot(
        pick_all, returned.reshape(total_slots, col_width), preferred_element_type=jnp.float32
    ).reshape(row_count, top_count, col_width)
    routed_sum = jnp.sum(route_weight[..., None] * fetched, axis=1)
    blended = (
        alpha_res * lax.dynamic_slice_in_dim(hidden, col_start, col_width, 1).astype(jnp.float32)
        + routed_sum
    )
    row_total, row_squares = lax.psum(
        (jnp.sum(blended, axis=1), jnp.sum(blended * blended, axis=1)), "tp"
    )
    row_mean = row_total / model_width
    spread = row_squares / model_width - row_mean * row_mean
    gain_part = lax.dynamic_slice_in_dim(norm_gain[1], col_start, col_width, 0)
    shift_part = lax.dynamic_slice_in_dim(norm_bias[1], col_start, col_width, 0)
    new_tokens = (
        (blended - row_mean[:, None]) * lax.rsqrt(spread[:, None] + eps_norm) * gain_part
        + shift_part
    ).astype(jnp.bfloat16)
    return (new_tokens, new_state)


def solution(mesh):
    in_specs = (
        P("ep", None),
        P("ep", "tp", None, None),
        P(None, "tp"),
        P(None, "tp"),
        P(None, "tp"),
        P(None, "tp"),
        P(None, "tp"),
        P(),
        P("tp", None),
        P(),
        P(),
        P(),
        P(),
        P("ep", None),
        P(("ep", "tp"), None, None),
        P(("ep", "tp"), None, None),
        P(("ep", "tp"), None, None),
    )
    out_specs = (P("ep", "tp"), P("ep", "tp", None, None))
    return jax.shard_map(
        on_device, mesh=mesh, in_specs=in_specs, out_specs=out_specs, check_vma=False
    )
```

profile of v0, /device:TPU:0, one launch (start us, length us, event | category | flops | bytes accessed | tf_op | source)
XLA Modules:
  0.0 94.1 jit_solution(932960176985230560)
XLA Ops:
  7.2 0.0 copy-start
  7.2 0.0 all-reduce.3.cloned.1.call-start
  7.2 1.7 %convolution_multiply_fusion.1 = f32[16,256]{1,0:T(8,128)S(1)} fusion(bf16[16,2048]{1,0:T(8,128)(2,1)} %param.17, bf16[2048,256]{1,0:T(8,128)(2,1)} %param.19), kind=kOutput, calls=%fused_computation.14 | convolution fusion | flops 16781312 | bytes 1130496 | tf_op jit(solution)/shard_map/dot_general | solution.py:41
  8.9 2.0 %fusion.42 = f32[16,512]{1,0:T(8,128)S(1)} fusion(bf16[16,2048]{1,0:T(8,128)(2,1)} %param.17, bf16[2048,512]{1,0:T(8,128)(2,1)} %param.22), kind=kOutput, calls=%fused_computation.83 | convolution fusion | flops 33554432 | bytes 2195456 | tf_op jit(solution)/shard_map/dot_general | solution.py:41
  11.0 0.2 fusion.41
  11.3 1.5 %fusion.25 = f32[16,256]{1,0:T(8,128)S(1)} fusion(bf16[16,2048]{1,0:T(8,128)(2,1)S(1)} %copy-done.1, bf16[2048,256]{1,0:T(8,128)(2,1)} %param.21), kind=kOutput, calls=%fused_computation.41 | convolution fusion | flops 16814080 | bytes 1130496 | tf_op jit(solution)/shard_map/dot_general | solution.py:41
  12.8 5.7 %multiply_reduce_fusion = (f32[16,2,256]{2,1,0:T(2,128)S(1)}, f32[16,2,128,256]{3,2,1,0:T(8,128)}) fusion(f32[16,2,128]{2,1,0:T(2,128)S(1)} %mul.188, f32[16,2,256]{2,1,0:T(2,128)S(1)} %mul.195, f32[16,2,128]{2,1,0:T(2,128)S(1)} %mul.193, f32[16,2,128,256]{3,2,1,0:T(8,128)} %param.18, f32[16,2,128]{2,1,0:T(2,128)S(1)} %mul.190), kind=kLoop, calls=%fused_computation | loop fusion | flops 5234688 | bytes 8503296 | tf_op jit(solution)/shard_map/reduce_sum | solution.py:53
  18.4 0.1 multiply_reduce_fusion.3
  18.6 0.1 broadcast_multiply_fusion
  18.7 3.0 %convolution_convert_fusion.2 = bf16[16,2048]{1,0:T(8,128)(2,1)} fusion(bf16[512,2048]{1,0:T(8,128)(2,1)S(1)} %copy-done, f32[16,512]{1,0:T(8,128)S(1)} %bitcast.96, f32[512]{0:T(512)S(1)} %bitcast.102, bf16[16,2048]{1,0:T(8,128)(2,1)S(1)} %copy-done.1, bf16[2048,512]{1,0:T(8,128)(2,1)} %param.23), kind=kOutput, calls=%fused_computation.5 | convolution fusion | flops 67198976 | bytes 4360192 | tf_op jit(solution)/shard_map/dot_general | solution.py:59
  21.7 0.0 all-reduce.3.cloned.1.call-update
  21.8 0.1 copy.52
  21.9 0.6 fusion.34
  22.4 0.1 eq.98
  22.5 0.1 fusion.27
  22.6 0.1 reduce_window_sum.11
  22.7 0.2 select_reduce_fusion
  22.9 0.1 reduce_sum.118
  23.0 0.8 fusion.10
  23.8 1.1 %reshape.146 = f32[16,2,32]{2,1,0:T(2,128)S(1)} reshape(f32[32,16,1,2]{3,1,0,2:T(8,128)} %fusion.10) | data formatting | bytes 8192 | tf_op jit(solution)/shard_map/rks,rd->sd/convert_element_type | solution.py:99
  24.9 0.1 copy.53
  25.0 0.6 multiply_add_fusion.3
  25.6 16.7 %all-reduce.3.cloned.1.call-done = bf16[16,2048]{1,0:T(8,128)(2,1)} async-done(((bf16[16,2048]{1,0:T(8,128)(2,1)}), bf16[16,2048]{1,0:T(8,128)(2,1)}) %all-reduce.3.cloned.1.call-update) | async-done | bytes 65552 | tf_op jit(solution)/shard_map/psum | solution.py:60
  42.4 1.0 %fusion.17 = f32[16]{0:T(128)S(1)} fusion(bf16[16,2048]{1,0:T(8,128)(2,1)} %all-reduce.3.cloned.1.call-done, bf16[16,2048]{1,0:T(8,128)(2,1)S(1)} %copy-done.1), kind=kLoop, calls=%fused_computation.27 | loop fusion | flops 163824 | bytes 131136 | tf_op jit(solution)/shard_map/reduce_sum | solution.py:11
  43.3 1.0 %multiply_reduce_fusion.1 = f32[16]{0:T(128)S(1)} fusion(bf16[16,2048]{1,0:T(8,128)(2,1)} %all-reduce.3.cloned.1.call-done, bf16[16,2048]{1,0:T(8,128)(2,1)S(1)} %copy-done.1, f32[16]{0:T(128)S(1)} %broadcast_multiply_fusion.2), kind=kLoop, calls=%fused_computation.23 | loop fusion | flops 229360 | bytes 131200 | tf_op jit(solution)/shard_map/reduce_sum | solution.py:12
  44.4 0.9 add_convert_fusion
  45.3 0.2 fusion.44
  45.5 0.7 reshape.139
  46.3 6.8 %all-to-all-start = ((bf16[16,1,2,2048]{3,2,1,0:T(2,128)(2,1)}), bf16[16,1,2,2048]{3,2,1,0:T(2,128)(2,1)S(1)}, u32[]{:S(2)}, u32[]{:S(2)}) async-start(bf16[16,1,2,2048]{3,2,1,0:T(2,128)(2,1)} %bitcast.4), calls=%async_computation | async-start | bytes 262144 | tf_op jit(solution)/shard_map/all_to_all | solution.py:108
  53.1 0.9 select_reduce_fusion.2
  54.0 0.1 fusion.43
  54.2 6.8 %all-to-all-done = bf16[16,1,2,2048]{3,2,1,0:T(2,128)(2,1)S(1)} async-done(((bf16[16,1,2,2048]{3,2,1,0:T(2,128)(2,1)}), bf16[16,1,2,2048]{3,2,1,0:T(2,128)(2,1)S(1)}, u32[]{:S(2)}, u32[]{:S(2)}) %all-to-all-start) | async-done | bytes 131104 | tf_op jit(solution)/shard_map/all_to_all | solution.py:108
  61.0 1.5 %convolution_bitcast_fusion.1 = f32[16,1,2,256]{3,0,2,1:T(8,128)S(1)} fusion(bf16[1,2048,256]{2,1,0:T(8,128)(2,1)} %param.31, bf16[16,1,2,2048]{3,2,1,0:T(2,128)(2,1)S(1)} %all-to-all-done), kind=kOutput, calls=%fused_computation.10 | convolution fusion | flops 33554432 | bytes 1212416 | tf_op jit(solution)/shard_map/secd,edf->secf/dot_general | solution.py:109
  62.5 2.0 %fusion = bf16[16,1,2,2048]{3,0,2,1:T(8,128)(2,1)S(1)} fusion(bf16[1,256,2048]{2,1,0:T(8,128)(2,1)S(1)} %copy-done.2, bf16[1,2048,256]{2,1,0:T(8,128)(2,1)} %param.32, bf16[16,1,2,2048]{3,2,1,0:T(2,128)(2,1)S(1)} %all-to-all-done, f32[16,1,2,256]{3,0,2,1:T(8,128)S(1)} %convolution_bitcast_fusion.1), kind=kOutput, calls=%fused_computation.4 | convolution fusion | flops 67223552 | bytes 2392064 | tf_op jit(solution)/shard_map/secf,efd->secd/dot_general | solution.py:114
  64.4 0.8 copy.56
  65.2 3.5 %all-to-all-start.1 = ((bf16[16,1,2,2048]{3,2,1,0:T(2,128)(2,1)}), bf16[16,1,2,2048]{3,2,1,0:T(2,128)(2,1)S(1)}, u32[]{:S(2)}, u32[]{:S(2)}) async-start(bf16[16,1,2,2048]{3,2,1,0:T(2,128)(2,1)} %copy.56), calls=%async_computation.1 | async-start | bytes 262144 | tf_op jit(solution)/shard_map/all_to_all | solution.py:118
  68.8 0.2 select_reduce_fusion.1
  69.0 7.6 %all-to-all-done.1 = bf16[16,1,2,2048]{3,2,1,0:T(2,128)(2,1)S(1)} async-done(((bf16[16,1,2,2048]{3,2,1,0:T(2,128)(2,1)}), bf16[16,1,2,2048]{3,2,1,0:T(2,128)(2,1)S(1)}, u32[]{:S(2)}, u32[]{:S(2)}) %all-to-all-start.1) | async-done | bytes 131104 | tf_op jit(solution)/shard_map/all_to_all | solution.py:118
  76.5 0.8 copy.57
  77.3 1.1 %reshape.152 = bf16[2,2,16384]{2,1,0:T(2,128)(2,1)S(1)} reshape(bf16[2048,1,2,16]{3,2,1,0:T(2,128)(2,1)S(1)} %bitcast.93) | data formatting | bytes 262144
  78.4 3.8 %all_to_all.25 = bf16[2,2,16384]{2,1,0:T(2,128)(2,1)S(1)} all-to-all(bf16[2,2,16384]{2,1,0:T(2,128)(2,1)S(1)} %reshape.152), channel_id=1, replica_groups=mesh['ep'=16,'tp'=2] {'tp'}, dimensions={0} | all-to-all | bytes 262144 | tf_op jit(solution)/shard_map/all_to_all | solution.py:117
  82.2 0.7 reshape.153
  82.9 0.8 copy.58
  83.7 0.1 reshape.150
  83.7 0.2 fusion.1
  84.0 0.1 fusion.32
  84.1 2.5 %all-reduce = (f32[16]{0:T(128)S(1)}, f32[16]{0:T(128)S(1)}) all-reduce(f32[16]{0:T(128)S(1)} %get-tuple-element.3, f32[16]{0:T(128)S(1)} %get-tuple-element.2), channel_id=1, replica_groups=mesh['ep'=16,'tp'=2] {'tp'}, use_global_device_ids=true, to_apply=%region_15.16 | all-reduce | flops 32 | bytes 256 | tf_op jit(solution)/shard_map/psum | solution.py:132
  86.6 0.7 add_convert_fusion.1
  (41 shorter events, 0.3 us)
Async XLA Ops:
  7.2 11.5 %copy-start = (bf16[512,2048]{1,0:T(8,128)(2,1)S(1)}, bf16[512,2048]{1,0:T(8,128)(2,1)}, u32[]{:S(2)}) copy-start(bf16[512,2048]{1,0:T(8,128)(2,1)} %param.25) | copy-start | bytes 6291460
  7.2 3.8 %copy-start.1 = (bf16[16,2048]{1,0:T(8,128)(2,1)S(1)}, bf16[16,2048]{1,0:T(8,128)(2,1)}, u32[]{:S(2)}) copy-start(bf16[16,2048]{1,0:T(8,128)(2,1)} %param.17) | copy-start | bytes 196612
  7.2 3.8 %copy-start.3 = (bf16[2048,256]{1,0:T(8,128)(2,1)S(1)}, bf16[2048,256]{1,0:T(8,128)(2,1)}, u32[]{:S(2)}) copy-start(bf16[2048,256]{1,0:T(8,128)(2,1)} %param.20) | copy-start | bytes 3145732
  7.2 35.2 %all-reduce.3.cloned.1.call-start = ((), (), s32[]{:S(2)}) async-start(), calls=%async_computation.3 | async-start | bytes 131072 | tf_op jit(solution)/shard_map/psum | solution.py:60
  12.8 5.9 %copy-start.9 = (f32[256]{0:T(256)S(1)}, f32[256]{0:T(256)}, u32[]{:S(2)}) copy-start(f32[256]{0:T(256)} %param.24) | copy-start | bytes 3076
  18.7 3.1 %copy-start.7 = (s32[16,2]{0,1:T(2,128)S(1)}, s32[16,2]{0,1:T(2,128)}, u32[]{:S(2)}) copy-start(s32[16,2]{0,1:T(2,128)} %param.30) | copy-start | bytes 388
  18.7 4.2 %copy-start.5 = (f32[2,2048]{1,0:T(2,128)S(1)}, f32[2,2048]{1,0:T(2,128)}, u32[]{:S(2)}) copy-start(f32[2,2048]{1,0:T(2,128)} %param.27) | copy-start | bytes 49156
  18.7 4.3 %copy-start.6 = (f32[2,2048]{1,0:T(2,128)S(1)}, f32[2,2048]{1,0:T(2,128)}, u32[]{:S(2)}) copy-start(f32[2,2048]{1,0:T(2,128)} %param.26) | copy-start | bytes 49156
  21.7 32.3 %copy-start.4 = (bf16[2048,32]{0,1:T(8,128)(2,1)S(1)}, bf16[2048,32]{0,1:T(8,128)(2,1)}, u32[]{:S(2)}) copy-start(bf16[2048,32]{0,1:T(8,128)(2,1)} %param.29) | copy-start | bytes 393220
  21.7 40.8 %copy-start.2 = (bf16[1,256,2048]{2,1,0:T(8,128)(2,1)S(1)}, bf16[1,256,2048]{2,1,0:T(8,128)(2,1)}, u32[]{:S(2)}) copy-start(bf16[1,256,2048]{2,1,0:T(8,128)(2,1)} %param.33) | copy-start | bytes 3145732
  46.3 14.7 %all-to-all-start = ((bf16[16,1,2,2048]{3,2,1,0:T(2,128)(2,1)}), bf16[16,1,2,2048]{3,2,1,0:T(2,128)(2,1)S(1)}, u32[]{:S(2)}, u32[]{:S(2)}) async-start(bf16[16,1,2,2048]{3,2,1,0:T(2,128)(2,1)} %bitcast.4), calls=%async_computation | async-start | bytes 262144 | tf_op jit(solution)/shard_map/all_to_all | solution.py:108
  65.2 11.3 %all-to-all-start.1 = ((bf16[16,1,2,2048]{3,2,1,0:T(2,128)(2,1)}), bf16[16,1,2,2048]{3,2,1,0:T(2,128)(2,1)S(1)}, u32[]{:S(2)}, u32[]{:S(2)}) async-start(bf16[16,1,2,2048]{3,2,1,0:T(2,128)(2,1)} %copy.56), calls=%async_computation.1 | async-start | bytes 262144 | tf_op jit(solution)/shard_map/all_to_all | solution.py:118
  77.3 6.5 %copy-start.8 = (s32[16,2]{0,1:T(2,128)S(1)}, s32[16,2]{0,1:T(2,128)}, u32[]{:S(2)}) copy-start(s32[16,2]{0,1:T(2,128)} %multiply_add_fusion.3) | copy-start | bytes 388
Sparse Core Ops, SparseCore 0:
  21.9 20.4 all-reduce.2
where the time goes:
time: 94.9 us; the launch traced here: 94.1 us
  waiting for transfers between devices  31.1 us (33%)
  between operations  14.4 us (15%)
  matrix products  13.3 us (14%)
  other arithmetic  12.1 us (13%)
  starting transfers between devices  10.4 us (11%)
  local copies, waits for them, and re-layouts  6.53 us (7%)
  blocking collectives  6.31 us (7%)
    psum x1, waiting for transfers between devices, on_device(): lax.psum(partial_value.astype(jnp.bfloat16), 'tp').astype(jnp.float32)  16.7 us
    all_to_all x1, waiting for transfers between devices, on_device(): lax.all_to_all(results, 'ep', split_axis=0, concat_axis=0, tiled=True)  7.57 us
    all_to_all x1, starting transfers between devices, on_device(): lax.all_to_all(outgoing, 'ep', split_axis=0, concat_axis=0, tiled=True)  6.83 us
    all_to_all x1, waiting for transfers between devices, on_device(): lax.all_to_all(outgoing, 'ep', split_axis=0, concat_axis=0, tiled=True)  6.8 us
    reduce_sum x1, other arithmetic, on_device(): readout = jnp.sum(queries[..., None] * new_state, axis=2)  5.65 us
    dot_general x4, matrix products, project(): return jnp.dot(tokens, weight, preferred_element_type=jnp.float32)  5.4 us
    all_to_all x1, blocking collectives, on_device(): lax.all_to_all(lax.all_to_all(results, 'ep', split_axis=0, concat_axis=0,...  3.84 us
    all_to_all x1, starting transfers between devices, on_device(): lax.all_to_all(results, 'ep', split_axis=0, concat_axis=0, tiled=True)  3.51 us
  transfers between devices with their start and end apart: 3, of which 3 were waited for; matrix products, arithmetic and copies ran while one was open for 5% of the time, Pallas kernels for 0%

commit v1 on v0

--- a/solution.py
+++ b/solution.py
@@ -5,6 +5,12 @@
 
 alpha_res = 2.0**0.5
 eps_norm = 1e-05
+
+
+def stacked_exchange(x, axis, split, join):
+    pieces = jnp.split(x, lax.axis_size(axis), axis=split)
+    incoming = lax.all_to_all(jnp.stack(pieces), axis, 0, 0)
+    return jnp.concatenate(incoming, axis=join)
 
 
 def layer_normed(inputs, gain_row, bias_row):
@@ -114,12 +120,8 @@
     results = jnp.einsum(
         "secf,efd->secd", activation, expert_down, preferred_element_type=jnp.float32
     ).astype(jnp.bfloat16)
-    returned = lax.all_to_all(
-        lax.all_to_all(results, "ep", split_axis=0, concat_axis=0, tiled=True),
-        "tp",
-        split_axis=3,
-        concat_axis=1,
-        tiled=True,
+    returned = stacked_exchange(
+        lax.all_to_all(results, "ep", split_axis=0, concat_axis=0, tiled=True), "tp", 3, 1
     )
     fetched = jnp.dot(
         pick_all, returned.reshape(total_slots, col_width), preferred_element_type=jnp.float32

time: 94.9 us -> 92 us (0.969)
  local copies, waits for them, and re-layouts: 6.53 us -> 2.49 us
  waiting for transfers between devices: 31.1 us -> 33 us
  other arithmetic: 12.1 us -> 10.5 us
    psum x1, waiting for transfers between devices: 16.7 us -> 19.5 us  [on_device(): lax.psum(partial_value.astype(jnp.bfloat16), 'tp').astype(jnp.float32)]
    unnamed x26 -> x20, local copies, waits for them, and re-layouts: 1.93 us -> 0.15 us
    all_to_all x2 -> x0, local copies, waits for them, and re-layouts: 1.51 us -> none  [the longest x1 0.76 us: on_device(): lax.all_to_all(results, 'ep', split_axis=0, concat_axis=0, tiled=True)]
  transfers between devices with their start and end apart: 3 -> 3, of which waited for: 3 -> 3; matrix products, arithmetic and copies ran while one was open for 5% -> 3% of each run, Pallas kernels for 0% -> 0%
where the time goes in v1:
time: 92 us; the launch traced here: 91.2 us
  waiting for transfers between devices  33 us (36%)
  between operations  14.4 us (16%)
  matrix products  14.2 us (15%)
  other arithmetic  10.5 us (11%)
  starting transfers between devices  10.4 us (11%)
  blocking collectives  6.31 us (7%)
  local copies, waits for them, and re-layouts  2.49 us (3%)
    psum x1, waiting for transfers between devices, on_device(): lax.psum(partial_value.astype(jnp.bfloat16), 'tp').astype(jnp.float32)  19.5 us
    all_to_all x1, waiting for transfers between devices, on_device(): lax.all_to_all(results, 'ep', split_axis=0, concat_axis=0, tiled=True)  7.57 us
    all_to_all x1, starting transfers between devices, on_device(): lax.all_to_all(outgoing, 'ep', split_axis=0, concat_axis=0, tiled=True)  6.83 us
    all_to_all x1, waiting for transfers between devices, on_device(): lax.all_to_all(outgoing, 'ep', split_axis=0, concat_axis=0, tiled=True)  5.89 us
    reduce_sum x1, other arithmetic, on_device(): readout = jnp.sum(queries[..., None] * new_state, axis=2)  5.65 us
    dot_general x4, matrix products, project(): return jnp.dot(tokens, weight, preferred_element_type=jnp.float32)  5.4 us
    all_to_all x1, blocking collectives, stacked_exchange(): incoming = lax.all_to_all(jnp.stack(pieces), axis, 0, 0)  3.84 us
    all_to_all x1, starting transfers between devices, on_device(): lax.all_to_all(results, 'ep', split_axis=0, concat_axis=0, tiled=True)  3.51 us
  transfers between devices with their start and end apart: 3, of which 3 were waited for; matrix products, arithmetic and copies ran while one was open for 3% of the time, Pallas kernels for 0%

profile of v1, /device:TPU:0, one launch (start us, length us, event | category | flops | bytes accessed | tf_op | source)
XLA Modules:
  0.0 91.2 jit_solution(15945548360208319777)
XLA Ops:
  7.2 0.0 copy-start
  7.2 0.0 copy-start.1
  7.2 0.0 all-reduce.3.cloned.1.call-start
  7.2 1.7 %convolution_multiply_fusion.1 = f32[16,256]{1,0:T(8,128)S(1)} fusion(bf16[16,2048]{1,0:T(8,128)(2,1)} %param.17, bf16[2048,256]{1,0:T(8,128)(2,1)} %param.19), kind=kOutput, calls=%fused_computation.14 | convolution fusion | flops 16781312 | bytes 1130496 | tf_op jit(solution)/shard_map/dot_general | solution.py:47
  8.9 2.0 %fusion.42 = f32[16,512]{1,0:T(8,128)S(1)} fusion(bf16[16,2048]{1,0:T(8,128)(2,1)} %param.17, bf16[2048,512]{1,0:T(8,128)(2,1)} %param.22), kind=kOutput, calls=%fused_computation.86 | convolution fusion | flops 33554432 | bytes 2195456 | tf_op jit(solution)/shard_map/dot_general | solution.py:47
  11.0 0.2 fusion.41
  11.3 1.5 %fusion.25 = f32[16,256]{1,0:T(8,128)S(1)} fusion(bf16[16,2048]{1,0:T(8,128)(2,1)S(1)} %copy-done.1, bf16[2048,256]{1,0:T(8,128)(2,1)} %param.21), kind=kOutput, calls=%fused_computation.44 | convolution fusion | flops 16814080 | bytes 1130496 | tf_op jit(solution)/shard_map/dot_general | solution.py:47
  12.8 0.0 copy-start.7
  12.8 5.7 %multiply_reduce_fusion = (f32[16,2,256]{2,1,0:T(2,128)S(1)}, f32[16,2,128,256]{3,2,1,0:T(8,128)}) fusion(f32[16,2,128]{2,1,0:T(2,128)S(1)} %mul.188, f32[16,2,256]{2,1,0:T(2,128)S(1)} %mul.195, f32[16,2,128]{2,1,0:T(2,128)S(1)} %mul.193, f32[16,2,128,256]{3,2,1,0:T(8,128)} %param.18, f32[16,2,128]{2,1,0:T(2,128)S(1)} %mul.190), kind=kLoop, calls=%fused_computation | loop fusion | flops 5234688 | bytes 8503296 | tf_op jit(solution)/shard_map/reduce_sum | solution.py:59
  18.4 0.1 multiply_reduce_fusion.3
  18.6 0.1 broadcast_multiply_fusion
  18.7 0.0 copy-start.6
  18.7 3.0 %convolution_convert_fusion.2 = bf16[16,2048]{1,0:T(8,128)(2,1)} fusion(bf16[512,2048]{1,0:T(8,128)(2,1)S(1)} %copy-done, f32[16,512]{1,0:T(8,128)S(1)} %bitcast.97, f32[512]{0:T(512)S(1)} %bitcast.103, bf16[16,2048]{1,0:T(8,128)(2,1)S(1)} %copy-done.1, bf16[2048,512]{1,0:T(8,128)(2,1)} %param.23), kind=kOutput, calls=%fused_computation.5 | convolution fusion | flops 67198976 | bytes 4360192 | tf_op jit(solution)/shard_map/dot_general | solution.py:65
  21.7 0.0 all-reduce.3.cloned.1.call-update
  21.8 0.1 copy.51
  21.9 0.1 eq.98
  21.9 0.1 fusion.27
  22.0 0.1 reduce_window_sum.11
  22.1 0.2 select_reduce_fusion
  22.3 0.1 reduce_sum.118
  22.4 0.0 copy-done.4
  22.5 0.1 fusion.10
  22.6 0.2 reshape.145
  22.7 0.1 copy.52
  22.9 19.5 %all-reduce.3.cloned.1.call-done = bf16[16,2048]{1,0:T(8,128)(2,1)} async-done(((bf16[16,2048]{1,0:T(8,128)(2,1)}), bf16[16,2048]{1,0:T(8,128)(2,1)}) %all-reduce.3.cloned.1.call-update) | async-done | bytes 65552 | tf_op jit(solution)/shard_map/psum | solution.py:66
  42.3 1.0 %fusion.17 = f32[16]{0:T(128)S(1)} fusion(bf16[16,2048]{1,0:T(8,128)(2,1)} %all-reduce.3.cloned.1.call-done, bf16[16,2048]{1,0:T(8,128)(2,1)S(1)} %copy-done.1), kind=kLoop, calls=%fused_computation.28 | loop fusion | flops 163824 | bytes 131136 | tf_op jit(solution)/shard_map/reduce_sum | solution.py:17
  43.3 1.0 %multiply_reduce_fusion.1 = f32[16]{0:T(128)S(1)} fusion(bf16[16,2048]{1,0:T(8,128)(2,1)} %all-reduce.3.cloned.1.call-done, bf16[16,2048]{1,0:T(8,128)(2,1)S(1)} %copy-done.1, f32[16]{0:T(128)S(1)} %broadcast_multiply_fusion.2), kind=kLoop, calls=%fused_computation.24 | loop fusion | flops 229360 | bytes 131200 | tf_op jit(solution)/shard_map/reduce_sum | solution.py:18
  44.4 0.9 %add_convert_fusion = bf16[16,2048]{1,0:T(8,128)(2,1)S(1)} fusion(bf16[16,2048]{1,0:T(8,128)(2,1)} %all-reduce.3.cloned.1.call-done, bf16[16,2048]{1,0:T(8,128)(2,1)S(1)} %copy-done.1, f32[2048]{0:T(1024)S(1)} %bitcast.99, f32[2048]{0:T(1024)S(1)} %bitcast.100, f32[16]{0:T(128)S(1)} %add_rsqrt_fusion.2, f32[16]{0:T(128)S(1)} %broadcast_multiply_fusion.2), kind=kLoop, calls=%fused_computation.23 | loop fusion | flops 294912 | bytes 213120 | tf_op jit(solution)/shard_map/convert_element_type | solution.py:69
  45.3 0.2 fusion.44
  45.5 0.7 reshape.138
  46.3 6.8 %all-to-all-start = ((bf16[16,1,2,2048]{3,2,1,0:T(2,128)(2,1)}), bf16[16,1,2,2048]{3,2,1,0:T(2,128)(2,1)S(1)}, u32[]{:S(2)}, u32[]{:S(2)}) async-start(bf16[16,1,2,2048]{3,2,1,0:T(2,128)(2,1)} %bitcast.4), calls=%async_computation | async-start | bytes 262144 | tf_op jit(solution)/shard_map/all_to_all | solution.py:114
  53.1 0.9 select_reduce_fusion.2
  54.0 1.1 %fusion.43 = f32[16,32]{1,0:T(8,128)S(1)} fusion(bf16[16,2048]{1,0:T(8,128)(2,1)S(1)} %add_convert_fusion, bf16[2048,32]{0,1:T(8,128)(2,1)} %param.29), kind=kOutput, calls=%fused_computation.87 | convolution fusion | flops 2097152 | bytes 198656 | tf_op jit(solution)/shard_map/dot_general | solution.py:75
  55.1 5.9 %all-to-all-done = bf16[16,1,2,2048]{3,2,1,0:T(2,128)(2,1)S(1)} async-done(((bf16[16,1,2,2048]{3,2,1,0:T(2,128)(2,1)}), bf16[16,1,2,2048]{3,2,1,0:T(2,128)(2,1)S(1)}, u32[]{:S(2)}, u32[]{:S(2)}) %all-to-all-start) | async-done | bytes 131104 | tf_op jit(solution)/shard_map/all_to_all | solution.py:114
  61.0 1.5 %convolution_bitcast_fusion.1 = f32[16,1,2,256]{3,0,2,1:T(8,128)S(1)} fusion(bf16[1,2048,256]{2,1,0:T(8,128)(2,1)} %param.31, bf16[16,1,2,2048]{3,2,1,0:T(2,128)(2,1)S(1)} %all-to-all-done), kind=kOutput, calls=%fused_computation.10 | convolution fusion | flops 33554432 | bytes 1212416 | tf_op jit(solution)/shard_map/secd,edf->secf/dot_general | solution.py:115
  62.5 2.0 %fusion = bf16[16,1,2,2048]{3,0,2,1:T(8,128)(2,1)S(1)} fusion(bf16[1,256,2048]{2,1,0:T(8,128)(2,1)S(1)} %copy-done.2, bf16[1,2048,256]{2,1,0:T(8,128)(2,1)} %param.32, bf16[16,1,2,2048]{3,2,1,0:T(2,128)(2,1)S(1)} %all-to-all-done, f32[16,1,2,256]{3,0,2,1:T(8,128)S(1)} %convolution_bitcast_fusion.1), kind=kOutput, calls=%fused_computation.4 | convolution fusion | flops 67223552 | bytes 2392064 | tf_op jit(solution)/shard_map/secf,efd->secd/dot_general | solution.py:120
  64.4 0.8 copy.55
  65.2 3.5 %all-to-all-start.1 = ((bf16[16,1,2,2048]{3,2,1,0:T(2,128)(2,1)}), bf16[16,1,2,2048]{3,2,1,0:T(2,128)(2,1)S(1)}, u32[]{:S(2)}, u32[]{:S(2)}) async-start(bf16[16,1,2,2048]{3,2,1,0:T(2,128)(2,1)} %copy.55), calls=%async_computation.1 | async-start | bytes 262144 | tf_op jit(solution)/shard_map/all_to_all | solution.py:124
  68.7 0.2 select_reduce_fusion.1
  68.9 7.6 %all-to-all-done.1 = bf16[16,1,2,2048]{3,2,1,0:T(2,128)(2,1)S(1)} async-done(((bf16[16,1,2,2048]{3,2,1,0:T(2,128)(2,1)}), bf16[16,1,2,2048]{3,2,1,0:T(2,128)(2,1)S(1)}, u32[]{:S(2)}, u32[]{:S(2)}) %all-to-all-start.1) | async-done | bytes 131104 | tf_op jit(solution)/shard_map/all_to_all | solution.py:124
  76.6 0.2 pad_maximum_fusion
  76.8 3.8 %all_to_all.15 = bf16[2,16,1,2,1024]{4,3,1,2,0:T(2,128)(2,1)S(1)} all-to-all(bf16[2,16,1,2,1024]{4,3,1,2,0:T(2,128)(2,1)S(1)} %pad_maximum_fusion), channel_id=1, replica_groups=mesh['ep'=16,'tp'=2] {'tp'}, dimensions={0} | all-to-all | bytes 262144 | tf_op jit(solution)/shard_map/all_to_all | solution.py:12
  80.6 0.1 copy.57
  80.7 0.1 reshape.149
  80.8 0.2 fusion.1
  81.0 0.1 fusion.32
  81.1 2.5 %all-reduce = (f32[16]{0:T(128)S(1)}, f32[16]{0:T(128)S(1)}) all-reduce(f32[16]{0:T(128)S(1)} %get-tuple-element.3, f32[16]{0:T(128)S(1)} %get-tuple-element.2), channel_id=1, replica_groups=mesh['ep'=16,'tp'=2] {'tp'}, use_global_device_ids=true, to_apply=%region_15.16 | all-reduce | flops 32 | bytes 256 | tf_op jit(solution)/shard_map/psum | solution.py:134
  83.6 0.7 add_convert_fusion.1
  (37 shorter events, 0.4 us)
Async XLA Ops:
  7.2 11.5 %copy-start = (bf16[512,2048]{1,0:T(8,128)(2,1)S(1)}, bf16[512,2048]{1,0:T(8,128)(2,1)}, u32[]{:S(2)}) copy-start(bf16[512,2048]{1,0:T(8,128)(2,1)} %param.25) | copy-start | bytes 6291460
  7.2 3.8 %copy-start.1 = (bf16[16,2048]{1,0:T(8,128)(2,1)S(1)}, bf16[16,2048]{1,0:T(8,128)(2,1)}, u32[]{:S(2)}) copy-start(bf16[16,2048]{1,0:T(8,128)(2,1)} %param.17) | copy-start | bytes 196612
  7.2 3.8 %copy-start.3 = (bf16[2048,256]{1,0:T(8,128)(2,1)S(1)}, bf16[2048,256]{1,0:T(8,128)(2,1)}, u32[]{:S(2)}) copy-start(bf16[2048,256]{1,0:T(8,128)(2,1)} %param.20) | copy-start | bytes 3145732
  7.2 35.1 %all-reduce.3.cloned.1.call-start = ((), (), s32[]{:S(2)}) async-start(), calls=%async_computation.3 | async-start | bytes 131072 | tf_op jit(solution)/shard_map/psum | solution.py:66
  12.8 5.9 %copy-start.7 = (f32[256]{0:T(256)S(1)}, f32[256]{0:T(256)}, u32[]{:S(2)}) copy-start(f32[256]{0:T(256)} %param.24) | copy-start | bytes 3076
  18.7 3.1 %copy-start.6 = (s32[16,2]{0,1:T(2,128)S(1)}, s32[16,2]{0,1:T(2,128)}, u32[]{:S(2)}) copy-start(s32[16,2]{0,1:T(2,128)} %param.30) | copy-start | bytes 388
  18.7 3.6 %copy-start.4 = (f32[2,2048]{1,0:T(2,128)S(1)}, f32[2,2048]{1,0:T(2,128)}, u32[]{:S(2)}) copy-start(f32[2,2048]{1,0:T(2,128)} %param.27) | copy-start | bytes 49156
  18.7 3.7 %copy-start.5 = (f32[2,2048]{1,0:T(2,128)S(1)}, f32[2,2048]{1,0:T(2,128)}, u32[]{:S(2)}) copy-start(f32[2,2048]{1,0:T(2,128)} %param.26) | copy-start | bytes 49156
  21.7 40.8 %copy-start.2 = (bf16[1,256,2048]{2,1,0:T(8,128)(2,1)S(1)}, bf16[1,256,2048]{2,1,0:T(8,128)(2,1)}, u32[]{:S(2)}) copy-start(bf16[1,256,2048]{2,1,0:T(8,128)(2,1)} %param.33) | copy-start | bytes 3145732
  46.3 14.7 %all-to-all-start = ((bf16[16,1,2,2048]{3,2,1,0:T(2,128)(2,1)}), bf16[16,1,2,2048]{3,2,1,0:T(2,128)(2,1)S(1)}, u32[]{:S(2)}, u32[]{:S(2)}) async-start(bf16[16,1,2,2048]{3,2,1,0:T(2,128)(2,1)} %bitcast.4), calls=%async_computation | async-start | bytes 262144 | tf_op jit(solution)/shard_map/all_to_all | solution.py:114
  65.2 11.3 %all-to-all-start.1 = ((bf16[16,1,2,2048]{3,2,1,0:T(2,128)(2,1)}), bf16[16,1,2,2048]{3,2,1,0:T(2,128)(2,1)S(1)}, u32[]{:S(2)}, u32[]{:S(2)}) async-start(bf16[16,1,2,2048]{3,2,1,0:T(2,128)(2,1)} %copy.55), calls=%async_computation.1 | async-start | bytes 262144 | tf_op jit(solution)/shard_map/all_to_all | solution.py:124
Sparse Core Ops, SparseCore 0:
  21.9 20.4 all-reduce.2
